TPU v7x, 32 devices: a whole 2x2x4 slice. The times are simulated.
32 devices in a mesh: ep: 8 (over z, x), tp: 4 (over y, core).
Axes of the slice: x: 2, y: 2, z: 4, core: 2. Of those that a mesh axis runs over, the one named last changes fastest.
Arguments:
- query_rows: bfloat16 [1536, 1024], P('ep', 'tp'), may hold values from -8 to 8
- key_rows: bfloat16 [1536, 1024], P('ep', 'tp'), may hold values from -8 to 8
- value_rows: bfloat16 [1536, 1024], P('ep', 'tp'), may hold values from -6 to 6
- lambdas: float32 [8], P('tp'), may hold values from 0.3 to 0.8
- head_gain: float32 [128], replicated, may hold values from 0.1 to 1.9
- w_out: bfloat16 [1024, 2048], replicated, may hold values from -0.1875 to 0.1875
- moe_rows: bfloat16 [4096, 2048], P('ep'), may hold values from -6 to 6
- ffn_gain: float32 [2048], replicated, may hold values from 0.1 to 1.9
- routes: int32 [4096, 2], P('ep'), may hold values from 0 to 7, all different within a row; in each aligned block of 128 rows (0 to 127, 128 to 255, ...) at most 64 rows name the same one
- group_logits: float32 [4096, 4], P('ep'), may hold values from -8 to 8
- pick_logits: float32 [4096, 2], P('ep'), may hold values from -8 to 8
- w_gate: bfloat16 [8, 2048, 1024], P('ep', None, 'tp'), may hold values from -0.125 to 0.125
- w_up: bfloat16 [8, 2048, 1024], P('ep', None, 'tp'), may hold values from -0.125 to 0.125
- w_down: bfloat16 [8, 1024, 2048], P('ep', 'tp'), may hold values from -0.75 to 0.75
Outputs:
- mixer_out: bfloat16 [1536, 2048], P(('ep', 'tp'))
- moe_out: bfloat16 [4096, 2048], P(('ep', 'tp'))
Inputs may be any that keep to these rules, and one draw needn't show every extreme that they name: `routes`: each row names 2 different experts. In each aligned block of 128 rows (the rows of one device) no expert is named by more than 64 rows; some expert is named by exactly 64 rows of a block.
All inputs are finite; a program needn't handle non-finite values.
Results may differ from a plain program's by a relative error of at most 0.015.
Values may be sent and summed in bfloat16 or wider, within the bound.
A program may use at most 128 MiB of HBM per device.

v0:
```python
import jax
import jax.numpy as jnp
from jax import lax
from jax.sharding import PartitionSpec as P

EPS = 1e-06
HEAD_SCALE = 0.8


def rms_rows(values, gain):
    squared = jnp.mean(values * values, axis=-1, keepdims=True)
    return values * lax.rsqrt(squared + EPS) * gain


def slot_index(picks, expert_count, capacity):
    flattened = picks.reshape(picks.shape[0], -1)
    onehot = (flattened[..., None] == jnp.arange(expert_count, dtype=jnp.int32)).astype(jnp.int32)
    before = jnp.cumsum(onehot, axis=1) - onehot
    ranking = jnp.sum(before * onehot, axis=-1)
    return flattened * capacity + ranking


def expert_hidden(arrived, gate_weight, up_weight):
    gate_part = jnp.dot(arrived, gate_weight, preferred_element_type=jnp.float32)
    up_part = jnp.dot(arrived, up_weight, preferred_element_type=jnp.float32)
    return (jax.nn.silu(gate_part) * up_part).astype(jnp.bfloat16)


def local(
    query_rows,
    key_rows,
    value_rows,
    lambdas,
    head_gain,
    w_out,
    moe_rows,
    ffn_gain,
    routes,
    group_logits,
    pick_logits,
    w_gate,
    w_up,
    w_down,
):
    token_count = query_rows.shape[0]
    local_heads = lambdas.shape[0]
    head_qk = query_rows.shape[1] // (2 * local_heads)
    head_v = value_rows.shape[1] // local_heads
    score_scale = head_qk ** (-0.5)
    queries = query_rows.reshape(token_count, local_heads, 2, head_qk)

    def absorb(carried, key_value):
        key_block, value_block = key_value
        running_max, running_sum, running_acc = carried
        scores = (
            jnp.einsum("qhmd,khmd->hmqk", queries, key_block, preferred_element_type=jnp.float32)
            * score_scale
        )
        new_max = jnp.maximum(running_max, jnp.max(scores, axis=-1))
        factor = jnp.exp(running_max - new_max)
        weights = jnp.exp(scores - new_max[..., None])
        running_sum = running_sum * factor + jnp.sum(weights, axis=-1)
        update = jnp.einsum(
            "hmqk,khv->hmqv",
            weights.astype(jnp.bfloat16),
            value_block,
            preferred_element_type=jnp.float32,
        )
        return ((new_max, running_sum, running_acc * factor[..., None] + update), None)

    start_state = (
        jnp.full((local_heads, 2, token_count), -1e30, jnp.float32),
        jnp.zeros((local_heads, 2, token_count), jnp.float32),
        jnp.zeros((local_heads, 2, token_count, head_v), jnp.float32),
    )
    carried = start_state
    key_piece = lax.all_gather(key_rows, "ep", axis=0, tiled=True)
    value_piece = lax.all_gather(value_rows, "ep", axis=0, tiled=True)
    length = key_piece.shape[0]
    block_rows = 1024 if length % 1024 == 0 else length
    blocks = (
        key_piece.reshape(length // block_rows, block_rows, local_heads, 2, head_qk),
        value_piece.reshape(length // block_rows, block_rows, local_heads, head_v),
    )
    carried, unused = lax.scan(absorb, carried, blocks)
    unused_max, final_sum, final_acc = carried
    averaged = final_acc / final_sum[..., None]
    per_head = averaged[:, 0] - lambdas[:, None, None] * averaged[:, 1]
    normed_heads = rms_rows(per_head, head_gain) * HEAD_SCALE
    attended = (
        jnp.transpose(normed_heads, (1, 0, 2))
        .reshape(token_count, local_heads * head_v)
        .astype(jnp.bfloat16)
    )
    own_weight = lax.dynamic_slice_in_dim(
        w_out, lax.axis_index("tp") * attended.shape[1], attended.shape[1], 0
    )
    mixer_out = lax.psum_scatter(
        jnp.dot(attended, own_weight, preferred_element_type=jnp.float32).astype(jnp.bfloat16),
        "tp",
        scatter_dimension=0,
        tiled=True,
    )
    quarters = lax.axis_size("tp")
    own_quarter = lax.axis_index("tp")
    expert_count = lax.axis_size("ep")
    model_width = moe_rows.shape[1]
    quarter_rows = moe_rows.shape[0] // quarters
    top_k = routes.shape[1]
    capacity = max(2, 2 * top_k * quarter_rows // expert_count)
    source_rows = jnp.repeat(jnp.arange(quarter_rows, dtype=jnp.int32), top_k)
    own_picks = lax.dynamic_slice_in_dim(routes, own_quarter * quarter_rows, quarter_rows, 0)
    own_tokens = lax.dynamic_slice_in_dim(moe_rows, own_quarter * quarter_rows, quarter_rows, 0)
    normed = rms_rows(own_tokens.astype(jnp.float32), ffn_gain).astype(jnp.bfloat16)
    own_slots = slot_index(own_picks[None], expert_count, capacity)[0]
    outgoing = (
        jnp.zeros((expert_count * capacity, model_width), jnp.bfloat16)
        .at[own_slots]
        .set(normed[source_rows])
    )
    arrived = lax.all_to_all(
        outgoing.reshape(expert_count, capacity, model_width),
        "ep",
        split_axis=0,
        concat_axis=0,
        tiled=True,
    )
    pieces = lax.all_gather(arrived, "tp", axis=0, tiled=True)
    flat_rows = pieces.reshape(-1, model_width)
    hidden = expert_hidden(flat_rows, w_gate[0], w_up[0]).reshape(pieces.shape[0], capacity, -1)
    hidden_flat = hidden.reshape(-1, hidden.shape[-1])
    summed = lax.psum_scatter(
        jnp.dot(hidden_flat, w_down[0], preferred_element_type=jnp.float32).astype(jnp.bfloat16),
        "tp",
        scatter_dimension=0,
        tiled=True,
    )
    returned = lax.all_to_all(
        summed.reshape(expert_count, capacity, model_width),
        "ep",
        split_axis=0,
        concat_axis=0,
        tiled=True,
    )
    picked = returned.reshape(-1, model_width)[own_slots].reshape(quarter_rows, top_k, model_width)
    own_groups = lax.dynamic_slice_in_dim(group_logits, own_quarter * quarter_rows, quarter_rows, 0)
    own_pick_logits = lax.dynamic_slice_in_dim(
        pick_logits, own_quarter * quarter_rows, quarter_rows, 0
    )
    group_count = group_logits.shape[1]
    group_prob = jax.nn.softmax(own_groups, axis=-1)
    group_index = own_picks // (expert_count // group_count)
    matches = (group_index[..., None] == jnp.arange(group_count, dtype=jnp.int32)).astype(
        jnp.float32
    )
    group_share = jnp.sum(group_prob[:, None, :] * matches, axis=-1)
    gate_values = group_share * jax.nn.softmax(own_pick_logits, axis=-1)
    moe_out = jnp.sum(gate_values[..., None] * picked.astype(jnp.float32), axis=1).astype(
        jnp.bfloat16
    )
    return (mixer_out, moe_out)


def solution(mesh):
    return jax.shard_map(
        local,
        mesh=mesh,
        in_specs=(
            P("ep", "tp"),
            P("ep", "tp"),
            P("ep", "tp"),
            P("tp"),
            P(),
            P(),
            P("ep", None),
            P(),
            P("ep", None),
            P("ep", None),
            P("ep", None),
            P("ep", None, "tp"),
            P("ep", None, "tp"),
            P("ep", "tp", None),
        ),
        out_specs=(P(("ep", "tp"), None), P(("ep", "tp"), None)),
        check_vma=False,
    )
```

profile of v0, /device:TPU:0, one launch (start us, length us, event | category | flops | bytes accessed | tf_op | source)
XLA Modules:
  0.0 339.7 jit_solution(261808291416860606)
XLA Ops:
  7.2 0.0 copy-start
  7.2 0.0 all-gather.2.cloned.1.call-start
  7.2 0.8 and_select_fusion
  8.0 0.1 copy.52
  8.1 0.1 eq.43
  8.3 0.6 reduce-window.6
  8.9 0.2 slice_reduce_fusion
  9.1 0.1 fusion.32
  9.2 0.1 copy.51
  9.3 0.1 mul.152
  9.5 0.1 reshape.255
  9.6 1.2 fusion.10
  10.9 2.0 fusion.12
  12.9 6.2 %scatter_custom_fusion = bf16[512,2048]{1,0:T(8,128)(2,1)S(1)} fusion(s32[256]{0:T(256)S(1)} %bitcast.82, bf16[128,2048]{1,0:T(8,128)(2,1)} %fusion.12, s32[1024]{0:T(1024)S(1)} %pad_clamp_fusion.1, bf16[]{:T(256)} %constant.73.clone.1), kind=kCustom, calls=%fused_computation.25 | custom fusion | bytes 2097664 | tf_op jit(solution)/shard_map/scatter | solution.py:119
  19.2 55.4 %all_to_all.10 = bf16[8,64,2048]{2,1,0:T(8,128)(2,1)} all-to-all(bf16[8,64,2048]{2,1,0:T(8,128)(2,1)S(1)} %bitcast.77), channel_id=1, replica_groups=mesh['ep'=8,'tp'=4] {'ep'}, dimensions={0} | all-to-all | bytes 4194304 | tf_op jit(solution)/shard_map/all_to_all | solution.py:121
  74.6 0.0 all-gather.2.cloned.1.call-update
  74.6 0.2 reduce-scatter.5.cloned.1.call-start
  74.9 57.2 %all-gather.2.cloned.1.call-done = bf16[32,64,2048]{2,1,0:T(8,128)(2,1)} async-done(((bf16[8,64,2048]{2,1,0:T(8,128)(2,1)}), bf16[32,64,2048]{2,1,0:T(8,128)(2,1)}) %all-gather.2.cloned.1.call-update) | async-done | bytes 8388624 | tf_op jit(solution)/shard_map/all_gather | solution.py:128
  132.1 0.0 copy-start.9
  132.1 7.4 %fusion.16 = f32[2048,256]{1,0:T(8,128)} fusion(bf16[2048,2048]{1,0:T(8,128)(2,1)} %bitcast.87, bf16[1,2048,256]{2,1,0:T(8,128)(2,1)} %param.25), kind=kOutput, calls=%fused_computation.23 | convolution fusion | flops 2147483648 | bytes 11534336 | tf_op jit(solution)/shard_map/dot_general | solution.py:24
  139.5 0.0 copy-done
  139.5 0.0 copy-done.9
  139.5 13.2 %convolution_convert_fusion = bf16[2048,2048]{1,0:T(8,128)(2,1)} fusion(bf16[2048,2048]{1,0:T(8,128)(2,1)} %bitcast.88, f32[2048,256]{1,0:T(8,128)} %fusion.16, bf16[1,256,2048]{2,1,0:T(8,128)(2,1)S(1)} %copy-done, bf16[1,2048,256]{2,1,0:T(8,128)(2,1)S(1)} %copy-done.9), kind=kOutput, calls=%fused_computation.3 | convolution fusion | flops 4302307328 | bytes 20971520 | tf_op jit(solution)/shard_map/dot_general | solution.py:133
  152.7 0.0 copy-start.2
  152.7 0.0 reduce-scatter.5.cloned.1.call-update
  152.7 0.9 copy-done.2
  153.5 0.0 copy-start.3
  153.6 32.4 %all_gather.9 = bf16[1536,256]{1,0:T(8,128)(2,1)S(1)} all-gather(bf16[192,256]{1,0:T(8,128)(2,1)S(1)} %copy-done.2), channel_id=1, replica_groups=mesh['ep'=8,'tp'=4] {'ep'}, dimensions={0}, use_global_device_ids=true | all-gather | bytes 884736 | tf_op jit(solution)/shard_map/all_gather | solution.py:77
  186.0 1.2 copy.45
  187.1 0.0 copy-done.3
  187.1 0.0 copy-start.4
  187.1 0.1 copy.44
  187.2 37.0 %reduce-scatter.5.cloned.1.call-done = bf16[512,2048]{1,0:T(8,128)(2,1)} async-done(((bf16[2048,2048]{1,0:T(8,128)(2,1)}), bf16[512,2048]{1,0:T(8,128)(2,1)}) %reduce-scatter.5.cloned.1.call-update) | async-done | bytes 2097168 | tf_op jit(solution)/shard_map/reduce_scatter | solution.py:132
  224.2 5.5 %all-to-all-start.1 = ((bf16[8,64,2048]{2,1,0:T(8,128)(2,1)}), bf16[8,64,2048]{2,1,0:T(8,128)(2,1)S(1)}, u32[]{:S(2)}, u32[]{:S(2)}) async-start(bf16[8,64,2048]{2,1,0:T(8,128)(2,1)} %bitcast.79), calls=%async_computation.3 | async-start | bytes 4194304 | tf_op jit(solution)/shard_map/all_to_all | solution.py:138
  229.7 0.0 reduce-scatter.3.cloned.1.call-start
  229.8 0.0 copy-done.4
  229.8 71.9 %all_gather.10 = bf16[1536,256]{1,0:T(8,128)(2,1)} all-gather(bf16[192,256]{1,0:T(8,128)(2,1)S(1)} %copy-done.4), channel_id=1, replica_groups=mesh['ep'=8,'tp'=4] {'ep'}, dimensions={0}, use_global_device_ids=true | all-gather | bytes 884736 | tf_op jit(solution)/shard_map/all_gather | solution.py:78
  301.7 2.3 copy.46
  304.0 2.0 multiply_reduce_fusion
  306.1 0.0 copy-start.1
  306.1 0.9 fusion
  307.0 0.2 copy-done.1
  307.2 0.0 copy-start.7
  307.2 0.0 copy-start.8
  307.2 1.2 fusion.23
  308.4 0.0 copy-done.7
  308.4 0.0 copy-start.5
  308.4 0.0 copy-start.6
  308.5 0.2 multiply_reduce_fusion.2
  308.7 0.0 copy-done.8
  308.7 2.6 convolution_convert_fusion.1
  311.3 0.0 reduce-scatter.3.cloned.1.call-update
  311.3 0.0 copy-done.5
  311.3 0.0 copy-done.6
  311.5 0.1 copy.50
  311.6 0.0 all-to-all-done.1
  311.6 2.3 gather_fusion
  314.0 2.4 reshape.260
  316.4 3.9 %multiply_reduce_fusion.1 = bf16[128,2048]{1,0:T(8,128)(2,1)} fusion(f32[128,2,2048]{2,1,0:T(2,128)S(1)} %reshape.260, f32[128,2]{1,0:T(8,128)S(1)} %copy.50), kind=kLoop, calls=%fused_computation.14 | loop fusion | flops 786432 | bytes 2622464 | tf_op jit(solution)/shard_map/reduce_sum | solution.py:158
  320.3 12.9 %reduce-scatter.3.cloned.1.call-done = bf16[48,2048]{1,0:T(8,128)(2,1)} async-done(((bf16[192,2048]{1,0:T(8,128)(2,1)}), bf16[48,2048]{1,0:T(8,128)(2,1)}) %reduce-scatter.3.cloned.1.call-update) | async-done | bytes 196624 | tf_op jit(solution)/shard_map/reduce_scatter | solution.py:98
  (19 shorter events, 0.3 us)
Async XLA Ops:
  7.2 132.3 %copy-start = (bf16[1,256,2048]{2,1,0:T(8,128)(2,1)S(1)}, bf16[1,256,2048]{2,1,0:T(8,128)(2,1)}, u32[]{:S(2)}) copy-start(bf16[1,256,2048]{2,1,0:T(8,128)(2,1)} %param.27) | copy-start | bytes 3145732
  7.2 124.9 %all-gather.2.cloned.1.call-start = ((), (), s32[]{:S(2)}) async-start(), calls=%async_computation.5 | async-start | bytes 10485760 | tf_op jit(solution)/shard_map/all_gather | solution.py:128
  74.6 149.6 %reduce-scatter.5.cloned.1.call-start = ((), (), s32[]{:S(2)}) async-start(), calls=%async_computation.6 | async-start | bytes 10485760 | tf_op jit(solution)/shard_map/reduce_scatter | solution.py:132
  132.1 7.4 %copy-start.9 = (bf16[1,2048,256]{2,1,0:T(8,128)(2,1)S(1)}, bf16[1,2048,256]{2,1,0:T(8,128)(2,1)}, u32[]{:S(2)}) copy-start(bf16[1,2048,256]{2,1,0:T(8,128)(2,1)} %param.26) | copy-start | bytes 3145732
  152.7 0.9 copy-start.2
  153.5 33.6 %copy-start.3 = (bf16[192,256]{1,0:T(8,128)(2,1)S(1)}, bf16[192,256]{1,0:T(8,128)(2,1)}, u32[]{:S(2)}) copy-start(bf16[192,256]{1,0:T(8,128)(2,1)} %param.14) | copy-start | bytes 294916
  187.1 42.6 %copy-start.4 = (bf16[192,256]{1,0:T(8,128)(2,1)S(1)}, bf16[192,256]{1,0:T(8,128)(2,1)}, u32[]{:S(2)}) copy-start(bf16[192,256]{1,0:T(8,128)(2,1)} %param.16) | copy-start | bytes 294916
  224.2 87.4 %all-to-all-start.1 = ((bf16[8,64,2048]{2,1,0:T(8,128)(2,1)}), bf16[8,64,2048]{2,1,0:T(8,128)(2,1)S(1)}, u32[]{:S(2)}, u32[]{:S(2)}) async-start(bf16[8,64,2048]{2,1,0:T(8,128)(2,1)} %bitcast.79), calls=%async_computation.3 | async-start | bytes 4194304 | tf_op jit(solution)/shard_map/all_to_all | solution.py:138
  229.7 103.5 %reduce-scatter.3.cloned.1.call-start = ((), (), s32[]{:S(2)}) async-start(), calls=%async_computation.4 | async-start | bytes 983040 | tf_op jit(solution)/shard_map/reduce_scatter | solution.py:98
  306.1 1.1 copy-start.1
  307.2 1.2 copy-start.7
  307.2 1.5 copy-start.8
  308.4 2.9 copy-start.5
  308.4 2.9 copy-start.6
Sparse Core Ops, SparseCore 0:
  74.7 57.2 all-gather.1
  152.8 71.3 reduce-scatter.4
  311.4 21.7 reduce-scatter.2
where the time goes:
time: 340 us
  blocking collectives  160 us (47%)
  waiting for transfers between devices  107 us (31%)
  matrix products  26.4 us (8%)
  local copies, waits for them, and re-layouts  16.6 us (5%)
  between operations  14 us (4%)
  other arithmetic  10 us (3%)
  starting transfers between devices  5.81 us (2%)
    all_gather x1, blocking collectives, local(): value_piece = lax.all_gather(value_rows, 'ep', axis=0, tiled=True)  71.9 us
    all_gather x1, waiting for transfers between devices, local(): pieces = lax.all_gather(arrived, 'tp', axis=0, tiled=True)  57.2 us
    all_to_all x1, blocking collectives, local(): lax.all_to_all(outgoing.reshape(expert_count, capacity, model_width), 'ep...  55.4 us
    reduce_scatter x1, waiting for transfers between devices, local(): lax.psum_scatter(jnp.dot(hidden_flat, w_down[0], preferred_element_type=j...  37 us
    all_gather x1, blocking collectives, local(): key_piece = lax.all_gather(key_rows, 'ep', axis=0, tiled=True)  32.4 us
    dot_general x1, matrix products, local(): jnp.dot(hidden_flat, w_down[0], preferred_element_type=jnp.float32)  13.2 us
    reduce_scatter x1, waiting for transfers between devices, local(): lax.psum_scatter(jnp.dot(attended, own_weight, preferred_element_type=jnp...  12.9 us
    dot_general x1, matrix products, expert_hidden(): jnp.dot(arrived, gate_weight, preferred_element_type=jnp.float32)  7.4 us
  transfers between devices with their start and end apart: 4, of which 3 were waited for; matrix products, arithmetic and copies ran while one was open for 6% of the time, Pallas kernels for 0%

commit v1 on v0

--- a/solution.py
+++ b/solution.py
@@ -75,7 +75,12 @@
     )
     carried = start_state
     key_piece = lax.all_gather(key_rows, "ep", axis=0, tiled=True)
-    value_piece = lax.all_gather(value_rows, "ep", axis=0, tiled=True)
+    ring = [value_rows]
+    for hop in range(7):
+        ring.append(lax.ppermute(ring[-1], "ep", [(dev, (dev + 1) % 8) for dev in range(8)]))
+    value_piece = jnp.roll(
+        jnp.concatenate(ring[::-1], axis=0), (lax.axis_index("ep") + 1) * ring[0].shape[0], axis=0
+    )
     length = key_piece.shape[0]
     block_rows = 1024 if length % 1024 == 0 else length
     blocks = (

time: 340 us -> 333 us (0.979)
  blocking collectives: 160 us -> 88.8 us
  waiting for transfers between devices: 107 us -> 160 us
  starting transfers between devices: 5.81 us -> 10.1 us
  local copies, waits for them, and re-layouts: 16.6 us -> 20.2 us
    all_gather x1 -> x0, blocking collectives: 71.9 us -> none  [local(): value_piece = lax.all_gather(value_rows, 'ep', axis=0, tiled=True)]
    ppermute x0 -> x7, waiting for transfers between devices: none -> 66.4 us  [local(): lax.ppermute(ring[-1], 'ep', [(dev, (dev + 1) % 8) for dev in range(8)])]
    reduce_scatter x1, waiting for transfers between devices: 37 us -> 18.5 us  [local(): lax.psum_scatter(jnp.dot(hidden_flat, w_down[0], preferred_element_type=j...]
    reduce_scatter x1, waiting for transfers between devices: 12.9 us -> 17.5 us  [local(): lax.psum_scatter(jnp.dot(attended, own_weight, preferred_element_type=jnp...]
    ppermute x0 -> x7, starting transfers between devices: none -> 4.29 us  [local(): lax.ppermute(ring[-1], 'ep', [(dev, (dev + 1) % 8) for dev in range(8)])]
    concatenate x0 -> x1, local copies, waits for them, and re-layouts: none -> 3.84 us  [local(): jnp.roll(jnp.concatenate(ring[::-1], axis=0), (lax.axis_index('ep') + 1)...]
  transfers between devices with their start and end apart: 4 -> 11, of which waited for: 3 -> 8; matrix products, arithmetic and copies ran while one was open for 6% -> 8% of each run, Pallas kernels for 0% -> 0%
where the time goes in v1:
time: 333 us; the launch traced here: 332 us
  waiting for transfers between devices  160 us (48%)
  blocking collectives  88.8 us (27%)
  matrix products  28.6 us (9%)
  local copies, waits for them, and re-layouts  20.2 us (6%)
  between operations  14 us (4%)
  other arithmetic  10.6 us (3%)
  starting transfers between devices  10.1 us (3%)
    ppermute x7, waiting for transfers between devices, local(): lax.ppermute(ring[-1], 'ep', [(dev, (dev + 1) % 8) for dev in range(8)])  66.4 us
    all_gather x1, waiting for transfers between devices, local(): pieces = lax.all_gather(arrived, 'tp', axis=0, tiled=True)  57.2 us
    all_to_all x1, blocking collectives, local(): lax.all_to_all(outgoing.reshape(expert_count, capacity, model_width), 'ep...  55.4 us
    all_gather x1, blocking collectives, local(): key_piece = lax.all_gather(key_rows, 'ep', axis=0, tiled=True)  33.4 us
    reduce_scatter x1, waiting for transfers between devices, local(): lax.psum_scatter(jnp.dot(hidden_flat, w_down[0], preferred_element_type=j...  18.5 us
    reduce_scatter x1, waiting for transfers between devices, local(): lax.psum_scatter(jnp.dot(attended, own_weight, preferred_element_type=jnp...  17.5 us
    dot_general x1, matrix products, local(): jnp.dot(hidden_flat, w_down[0], preferred_element_type=jnp.float32)  13.2 us
    dot_general x1, matrix products, expert_hidden(): jnp.dot(arrived, gate_weight, preferred_element_type=jnp.float32)  7.4 us
  transfers between devices with their start and end apart: 11, of which 8 were waited for; matrix products, arithmetic and copies ran while one was open for 8% of the time, Pallas kernels for 0%

profile of v1, /device:TPU:0, one launch (start us, length us, event | category | flops | bytes accessed | tf_op | source)
XLA Modules:
  0.0 332.0 jit_solution(13104202362934468836)
XLA Ops:
  7.2 0.0 copy-start
  7.2 0.0 all-gather.2.cloned.1.call-start
  7.2 0.8 and_select_fusion
  8.0 0.1 copy.58
  8.1 0.1 eq.46
  8.3 0.6 reduce-window.6
  8.9 0.2 slice_reduce_fusion
  9.1 0.1 fusion.32
  9.2 0.1 copy.57
  9.3 0.1 mul.156
  9.5 0.1 reshape.255
  9.6 1.2 fusion.10
  10.9 2.0 fusion.12
  12.9 6.2 %scatter_custom_fusion = bf16[512,2048]{1,0:T(8,128)(2,1)S(1)} fusion(s32[256]{0:T(256)S(1)} %bitcast.82, bf16[128,2048]{1,0:T(8,128)(2,1)} %fusion.12, s32[1024]{0:T(1024)S(1)} %pad_clamp_fusion.1, bf16[]{:T(256)} %constant.99.clone.1), kind=kCustom, calls=%fused_computation.25 | custom fusion | bytes 2097664 | tf_op jit(solution)/shard_map/scatter | solution.py:124
  19.2 55.4 %all_to_all.10 = bf16[8,64,2048]{2,1,0:T(8,128)(2,1)} all-to-all(bf16[8,64,2048]{2,1,0:T(8,128)(2,1)S(1)} %bitcast.77), channel_id=1, replica_groups=mesh['ep'=8,'tp'=4] {'ep'}, dimensions={0} | all-to-all | bytes 4194304 | tf_op jit(solution)/shard_map/all_to_all | solution.py:126
  74.6 0.0 all-gather.2.cloned.1.call-update
  74.6 0.2 reduce-scatter.5.cloned.1.call-start
  74.9 57.2 %all-gather.2.cloned.1.call-done = bf16[32,64,2048]{2,1,0:T(8,128)(2,1)} async-done(((bf16[8,64,2048]{2,1,0:T(8,128)(2,1)}), bf16[32,64,2048]{2,1,0:T(8,128)(2,1)}) %all-gather.2.cloned.1.call-update) | async-done | bytes 8388624 | tf_op jit(solution)/shard_map/all_gather | solution.py:133
  132.1 7.4 %fusion.16 = f32[2048,256]{1,0:T(8,128)} fusion(bf16[2048,2048]{1,0:T(8,128)(2,1)} %bitcast.87, bf16[1,2048,256]{2,1,0:T(8,128)(2,1)} %param.25), kind=kOutput, calls=%fused_computation.23 | convolution fusion | flops 2147483648 | bytes 11534336 | tf_op jit(solution)/shard_map/dot_general | solution.py:24
  139.5 13.2 %convolution_convert_fusion = bf16[2048,2048]{1,0:T(8,128)(2,1)} fusion(bf16[2048,2048]{1,0:T(8,128)(2,1)} %bitcast.88, f32[2048,256]{1,0:T(8,128)} %fusion.16, bf16[1,256,2048]{2,1,0:T(8,128)(2,1)S(1)} %copy-done, bf16[1,2048,256]{2,1,0:T(8,128)(2,1)S(1)} %copy-done.10), kind=kOutput, calls=%fused_computation.3 | convolution fusion | flops 4302307328 | bytes 20971520 | tf_op jit(solution)/shard_map/dot_general | solution.py:138
  152.7 0.0 reduce-scatter.5.cloned.1.call-update
  152.7 0.9 copy-done.3
  153.6 0.1 copy.50
  153.7 1.5 collective-permute-start
  155.2 6.9 %collective-permute-done = bf16[192,256]{0,1:T(8,128)(2,1)S(1)} collective-permute-done((bf16[192,256]{0,1:T(8,128)(2,1)S(1)}, bf16[192,256]{0,1:T(8,128)(2,1)S(1)}, u32[]{:S(2)}, u32[]{:S(2)}) %collective-permute-start) | collective-permute-done | bytes 98336 | tf_op jit(solution)/shard_map/ppermute | solution.py:80
  162.1 0.0 collective-permute-start.1
  162.1 7.7 %collective-permute-done.1 = bf16[192,256]{0,1:T(8,128)(2,1)S(1)} collective-permute-done((bf16[192,256]{0,1:T(8,128)(2,1)S(1)}, bf16[192,256]{0,1:T(8,128)(2,1)S(1)}, u32[]{:S(2)}, u32[]{:S(2)}) %collective-permute-start.1) | collective-permute-done | bytes 98336 | tf_op jit(solution)/shard_map/ppermute | solution.py:80
  169.7 0.0 collective-permute-start.2
  169.7 33.4 %all_gather.6 = bf16[1536,256]{1,0:T(8,128)(2,1)S(1)} all-gather(bf16[192,256]{1,0:T(8,128)(2,1)S(1)} %copy-done.4), channel_id=1, replica_groups=mesh['ep'=8,'tp'=4] {'ep'}, dimensions={0}, use_global_device_ids=true | all-gather | bytes 884736 | tf_op jit(solution)/shard_map/all_gather | solution.py:77
  203.1 1.2 copy.49
  204.3 0.8 copy.48
  205.0 0.0 collective-permute-done.2
  205.0 0.7 collective-permute-start.3
  205.8 18.5 %reduce-scatter.5.cloned.1.call-done = bf16[512,2048]{1,0:T(8,128)(2,1)} async-done(((bf16[2048,2048]{1,0:T(8,128)(2,1)}), bf16[512,2048]{1,0:T(8,128)(2,1)}) %reduce-scatter.5.cloned.1.call-update) | async-done | bytes 2097168 | tf_op jit(solution)/shard_map/reduce_scatter | solution.py:137
  224.2 5.5 %all-to-all-start.1 = ((bf16[8,64,2048]{2,1,0:T(8,128)(2,1)}), bf16[8,64,2048]{2,1,0:T(8,128)(2,1)S(1)}, u32[]{:S(2)}, u32[]{:S(2)}) async-start(bf16[8,64,2048]{2,1,0:T(8,128)(2,1)} %bitcast.79), calls=%async_computation.3 | async-start | bytes 4194304 | tf_op jit(solution)/shard_map/all_to_all | solution.py:143
  229.7 0.0 reduce-scatter.3.cloned.1.call-start
  229.8 2.1 multiply_reduce_fusion
  231.9 0.0 collective-permute-done.3
  231.9 2.0 collective-permute-start.4
  234.0 37.4 %collective-permute-done.4 = bf16[192,256]{0,1:T(8,128)(2,1)S(1)} collective-permute-done((bf16[192,256]{0,1:T(8,128)(2,1)}, bf16[192,256]{0,1:T(8,128)(2,1)S(1)}, u32[]{:S(2)}, u32[]{:S(2)}) %collective-permute-start.4) | collective-permute-done | bytes 98336 | tf_op jit(solution)/shard_map/ppermute | solution.py:80
  271.4 0.0 collective-permute-start.5
  271.4 0.9 fusion
  272.3 6.9 %collective-permute-done.5 = bf16[192,256]{0,1:T(8,128)(2,1)} collective-permute-done((bf16[192,256]{0,1:T(8,128)(2,1)S(1)}, bf16[192,256]{0,1:T(8,128)(2,1)}, u32[]{:S(2)}, u32[]{:S(2)}) %collective-permute-start.5) | collective-permute-done | bytes 98336 | tf_op jit(solution)/shard_map/ppermute | solution.py:80
  279.2 0.0 collective-permute-start.6
  279.2 0.6 exponential_multiply_fusion
  279.8 7.5 %collective-permute-done.6 = bf16[192,256]{0,1:T(8,128)(2,1)} collective-permute-done((bf16[192,256]{0,1:T(8,128)(2,1)}, bf16[192,256]{0,1:T(8,128)(2,1)}, u32[]{:S(2)}, u32[]{:S(2)}) %collective-permute-start.6) | collective-permute-done | bytes 98336 | tf_op jit(solution)/shard_map/ppermute | solution.py:80
  287.3 3.8 %concatenate.6 = bf16[3072,256]{0,1:T(8,128)(2,1)} concatenate(bf16[192,256]{0,1:T(8,128)(2,1)} %collective-permute-done.6, bf16[192,256]{0,1:T(8,128)(2,1)} %collective-permute-done.5, bf16[192,256]{0,1:T(8,128)(2,1)} %copy-done.2, bf16[192,256]{0,1:T(8,128)(2,1)} %collective-permute-done.3, bf16[192,256]{0,1:T(8,128)(2,1)} %collective-permute-done.2, ...), dimensions={0} | concatenate | bytes 3145728 | tf_op jit(solution)/shard_map/jit(_roll_dynamic)/concatenate | solution.py:81
  291.2 1.5 constant_dynamic-slice_fusion.3
  292.6 0.0 copy-start.8
  292.6 0.0 copy-start.9
  292.7 3.4 %fusion.23 = f32[2,2,192,128]{3,2,1,0:T(8,128)S(1)} fusion(bf16[1536,2,128,1]{0,2,3,1:T(8,128)(2,1)S(1)} %bitcast.80, f32[2,2,192,1536]{3,2,1,0:T(8,128)} %copy-done.1, f32[2,2,192]{2,1,0:T(2,128)S(1)} %broadcast_maximum_fusion, f32[2,2,192]{2,1,0:T(2,128)} %get-tuple-element.19, f32[2,2,192]{2,1,0:T(2,128)S(1)} %get-tuple-element.18), kind=kOutput, calls=%fused_computation.30 | convolution fusion | flops 305725440 | bytes 5907456 | tf_op jit(solution)/shard_map/while/body/eval_jaxpr/hmqk,khv->hmqv/dot_general | solution.py:63
  296.0 0.0 copy-done.8
  296.0 0.0 copy-start.6
  296.0 0.0 copy-start.7
  296.1 0.2 multiply_reduce_fusion.2
  296.3 2.6 convolution_convert_fusion.1
  298.9 0.0 reduce-scatter.3.cloned.1.call-update
  298.9 0.0 copy-done.6
  299.1 0.1 copy.56
  299.2 0.0 all-to-all-done.1
  299.2 2.3 gather_fusion
  301.6 2.4 reshape.260
  304.0 3.9 %multiply_reduce_fusion.1 = bf16[128,2048]{1,0:T(8,128)(2,1)} fusion(f32[128,2,2048]{2,1,0:T(2,128)S(1)} %reshape.260, f32[128,2]{1,0:T(8,128)S(1)} %copy.56), kind=kLoop, calls=%fused_computation.14 | loop fusion | flops 786432 | bytes 2622464 | tf_op jit(solution)/shard_map/reduce_sum | solution.py:163
  307.9 17.5 %reduce-scatter.3.cloned.1.call-done = bf16[48,2048]{1,0:T(8,128)(2,1)} async-done(((bf16[192,2048]{1,0:T(8,128)(2,1)}), bf16[48,2048]{1,0:T(8,128)(2,1)}) %reduce-scatter.3.cloned.1.call-update) | async-done | bytes 196624 | tf_op jit(solution)/shard_map/reduce_scatter | solution.py:103
  (32 shorter events, 0.3 us)
Async XLA Ops:
  7.2 132.3 %copy-start = (bf16[1,256,2048]{2,1,0:T(8,128)(2,1)S(1)}, bf16[1,256,2048]{2,1,0:T(8,128)(2,1)}, u32[]{:S(2)}) copy-start(bf16[1,256,2048]{2,1,0:T(8,128)(2,1)} %param.27) | copy-start | bytes 3145732
  7.2 124.9 %all-gather.2.cloned.1.call-start = ((), (), s32[]{:S(2)}) async-start(), calls=%async_computation.5 | async-start | bytes 10485760 | tf_op jit(solution)/shard_map/all_gather | solution.py:133
  74.6 149.6 %reduce-scatter.5.cloned.1.call-start = ((), (), s32[]{:S(2)}) async-start(), calls=%async_computation.6 | async-start | bytes 10485760 | tf_op jit(solution)/shard_map/reduce_scatter | solution.py:137
  132.1 7.4 %copy-start.10 = (bf16[1,2048,256]{2,1,0:T(8,128)(2,1)S(1)}, bf16[1,2048,256]{2,1,0:T(8,128)(2,1)}, u32[]{:S(2)}) copy-start(bf16[1,2048,256]{2,1,0:T(8,128)(2,1)} %param.26) | copy-start | bytes 3145732
  152.7 0.9 copy-start.3
  152.7 17.1 %copy-start.4 = (bf16[192,256]{1,0:T(8,128)(2,1)S(1)}, bf16[192,256]{1,0:T(8,128)(2,1)}, u32[]{:S(2)}) copy-start(bf16[192,256]{1,0:T(8,128)(2,1)} %param.15) | copy-start | bytes 294916
  153.5 50.7 %copy-start.5 = (bf16[192,256]{1,0:T(8,128)(2,1)S(1)}, bf16[192,256]{1,0:T(8,128)(2,1)}, u32[]{:S(2)}) copy-start(bf16[192,256]{1,0:T(8,128)(2,1)} %param.14) | copy-start | bytes 294916
  153.7 8.4 %collective-permute-start = (bf16[192,256]{0,1:T(8,128)(2,1)S(1)}, bf16[192,256]{0,1:T(8,128)(2,1)S(1)}, u32[]{:S(2)}, u32[]{:S(2)}) collective-permute-start(bf16[192,256]{0,1:T(8,128)(2,1)S(1)} %copy.50), channel_id=1, source_target_pairs={{0,4},{4,8},{8,12},{12,16},{16,20},{20,24},{24,28},{28,0},{1,5},{5... | collective-permute-start | bytes 294920 | tf_op jit(solution)/shard_map/ppermute | solution.py:80
  162.1 7.7 %collective-permute-start.1 = (bf16[192,256]{0,1:T(8,128)(2,1)S(1)}, bf16[192,256]{0,1:T(8,128)(2,1)S(1)}, u32[]{:S(2)}, u32[]{:S(2)}) collective-permute-start(bf16[192,256]{0,1:T(8,128)(2,1)S(1)} %collective-permute-done), channel_id=1, source_target_pairs={{0,4},{4,8},{8,12},{12,16},{16,20},{20,24},{24,28},{28,0},{1,5},{5... | collective-permute-start | bytes 294920 | tf_op jit(solution)/shard_map/ppermute | solution.py:80
  169.7 35.3 %collective-permute-start.2 = (bf16[192,256]{0,1:T(8,128)(2,1)S(1)}, bf16[192,256]{0,1:T(8,128)(2,1)}, u32[]{:S(2)}, u32[]{:S(2)}) collective-permute-start(bf16[192,256]{0,1:T(8,128)(2,1)S(1)} %collective-permute-done.1), channel_id=1, source_target_pairs={{0,4},{4,8},{8,12},{12,16},{16,20},{20,24},{24,28},{28,0},{1,5},{5... | collective-permute-start | bytes 294920 | tf_op jit(solution)/shard_map/ppermute | solution.py:80
  205.0 26.9 %collective-permute-start.3 = (bf16[192,256]{0,1:T(8,128)(2,1)}, bf16[192,256]{0,1:T(8,128)(2,1)}, u32[]{:S(2)}, u32[]{:S(2)}) collective-permute-start(bf16[192,256]{0,1:T(8,128)(2,1)} %collective-permute-done.2), channel_id=1, source_target_pairs={{0,4},{4,8},{8,12},{12,16},{16,20},{20,24},{24,28},{28,0},{1,5},{5... | collective-permute-start | bytes 294920 | tf_op jit(solution)/shard_map/ppermute | solution.py:80
  224.2 75.0 %all-to-all-start.1 = ((bf16[8,64,2048]{2,1,0:T(8,128)(2,1)}), bf16[8,64,2048]{2,1,0:T(8,128)(2,1)S(1)}, u32[]{:S(2)}, u32[]{:S(2)}) async-start(bf16[8,64,2048]{2,1,0:T(8,128)(2,1)} %bitcast.79), calls=%async_computation.3 | async-start | bytes 4194304 | tf_op jit(solution)/shard_map/all_to_all | solution.py:143
  229.7 95.7 %reduce-scatter.3.cloned.1.call-start = ((), (), s32[]{:S(2)}) async-start(), calls=%async_computation.4 | async-start | bytes 983040 | tf_op jit(solution)/shard_map/reduce_scatter | solution.py:103
  231.9 40.4 %copy-start.1 = (f32[2,2,192,1536]{3,2,1,0:T(8,128)}, f32[2,2,192,1536]{3,2,1,0:T(8,128)S(1)}, u32[]{:S(2)}) copy-start(f32[2,2,192,1536]{3,2,1,0:T(8,128)S(1)} %get-tuple-element.28) | copy-start | bytes 14155780
  231.9 39.4 %collective-permute-start.4 = (bf16[192,256]{0,1:T(8,128)(2,1)}, bf16[192,256]{0,1:T(8,128)(2,1)S(1)}, u32[]{:S(2)}, u32[]{:S(2)}) collective-permute-start(bf16[192,256]{0,1:T(8,128)(2,1)} %collective-permute-done.3), channel_id=1, source_target_pairs={{0,4},{4,8},{8,12},{12,16},{16,20},{20,24},{24,28},{28,0},{1,5},{5... | collective-permute-start | bytes 294920 | tf_op jit(solution)/shard_map/ppermute | solution.py:80
  271.4 7.9 %copy-start.2 = (bf16[192,256]{0,1:T(8,128)(2,1)}, bf16[192,256]{0,1:T(8,128)(2,1)S(1)}, u32[]{:S(2)}) copy-start(bf16[192,256]{0,1:T(8,128)(2,1)S(1)} %collective-permute-done.4) | copy-start | bytes 294916
  271.4 7.9 %collective-permute-start.5 = (bf16[192,256]{0,1:T(8,128)(2,1)S(1)}, bf16[192,256]{0,1:T(8,128)(2,1)}, u32[]{:S(2)}, u32[]{:S(2)}) collective-permute-start(bf16[192,256]{0,1:T(8,128)(2,1)S(1)} %collective-permute-done.4), channel_id=1, source_target_pairs={{0,4},{4,8},{8,12},{12,16},{16,20},{20,24},{24,28},{28,0},{1,5},{5... | collective-permute-start | bytes 294920 | tf_op jit(solution)/shard_map/ppermute | solution.py:80
  279.2 8.1 %collective-permute-start.6 = (bf16[192,256]{0,1:T(8,128)(2,1)}, bf16[192,256]{0,1:T(8,128)(2,1)}, u32[]{:S(2)}, u32[]{:S(2)}) collective-permute-start(bf16[192,256]{0,1:T(8,128)(2,1)} %collective-permute-done.5), channel_id=1, source_target_pairs={{0,4},{4,8},{8,12},{12,16},{16,20},{20,24},{24,28},{28,0},{1,5},{5... | collective-permute-start | bytes 294920 | tf_op jit(solution)/shard_map/ppermute | solution.py:80
  292.6 3.4 %copy-start.8 = (f32[2]{0:T(128)S(1)}, f32[2]{0:T(128)}, u32[]{:S(2)}) copy-start(f32[2]{0:T(128)} %param.17) | copy-start | bytes 28
  292.6 3.6 %copy-start.9 = (f32[128]{0:T(128)S(1)}, f32[128]{0:T(128)}, u32[]{:S(2)}) copy-start(f32[128]{0:T(128)} %param.18) | copy-start | bytes 1540
  296.0 2.9 copy-start.6
  296.0 2.9 copy-start.7
Sparse Core Ops, SparseCore 0:
  74.7 57.2 all-gather.1
  152.8 71.3 reduce-scatter.4
  299.0 26.3 reduce-scatter.2
